TPU v7x, 32 devices: a whole 2x2x4 slice. The times are simulated.
32 devices in a mesh: sp: 4 (over x, core), tp: 8 (over z, y).
Axes of the slice: x: 2, y: 2, z: 4, core: 2. Of those that a mesh axis runs over, the one named last changes fastest.
Arguments:
- latents: bfloat16 [1024, 2048], P(('sp', 'tp')), may hold values from -6 to 6
- context: bfloat16 [256, 2048], P('sp'), may hold values from -6 to 6
- condition: float32 [2048], P('sp'), may hold values from -12 to 12
- context_condition: float32 [2048], P('sp'), may hold values from -12 to 12
- norm_gain: float32 [2048], replicated, may hold values from 0.1 to 1.9
- shift_weight: bfloat16 [2048, 2048], P('sp', 'tp'), may hold values from -0.09375 to 0.09375
- scale_weight: bfloat16 [2048, 2048], P('sp', 'tp'), may hold values from -0.09375 to 0.09375
- gate_weight: bfloat16 [2048, 2048], P('sp', 'tp'), may hold values from -0.125 to 0.125
- query_weight: bfloat16 [2048, 1024], P(None, 'tp'), may hold values from -0.125 to 0.125
- key_weight: bfloat16 [2048, 1024], P(None, 'tp'), may hold values from -0.125 to 0.125
- value_weight: bfloat16 [2048, 1024], P(None, 'tp'), may hold values from -0.125 to 0.125
- subtract_share: float32 [8], P('tp'), may hold values from 0.3 to 0.8
- head_gain: float32 [128], replicated, may hold values from 0.1 to 1.9
- output_weight: bfloat16 [1024, 2048], P('tp'), may hold values from -0.1875 to 0.1875
Outputs:
- updated: bfloat16 [1024, 2048], P(('sp', 'tp'))
All inputs are finite; a program needn't handle non-finite values.
Results may differ from a plain program's by a relative error of at most 0.013.
Values may be sent and summed in bfloat16 or wider, within the bound.
A program may use at most 64 MiB of HBM per device.

v0:
```python
import jax
import jax.numpy as jnp
from jax import lax
from jax.sharding import PartitionSpec as P

HEAD = 64
VALUE = 128
GRID_W = 64


norm_eps = 1e-06
head_eps = 1e-05
rope_theta = 10000.0
head_scale = 0.8


def rotary_tables(positions):
    quarter = HEAD // 4
    inverse = rope_theta ** (-2.0 * jnp.arange(quarter, dtype=jnp.float32) / (HEAD // 2))
    row_angle = (positions // GRID_W).astype(jnp.float32)[:, None] * inverse[None, :]
    column_angle = (positions % GRID_W).astype(jnp.float32)[:, None] * inverse[None, :]
    angles = jnp.concatenate([row_angle, row_angle, column_angle, column_angle], axis=-1)
    return (jnp.cos(angles), jnp.sin(angles))


def rotate(vectors, cosine, sine_table):
    quarter = HEAD // 4
    pieces = vectors.reshape(vectors.shape[:-1] + (2, 2, quarter))
    turned = jnp.concatenate([-pieces[..., 1:, :], pieces[..., :1, :]], axis=-2).reshape(
        vectors.shape
    )
    return vectors * cosine[:, None, :] + turned * sine_table[:, None, :]


def modulate(token_rows, gain_row, shift_row, scale_row):
    widened = token_rows.astype(jnp.float32)
    normed = widened * lax.rsqrt(jnp.mean(widened * widened, axis=-1, keepdims=True) + norm_eps)
    return (normed * gain_row * (1.0 + scale_row) + shift_row).astype(jnp.bfloat16)


def shards(
    latents,
    context,
    condition,
    context_condition,
    norm_gain,
    shift_weight,
    scale_weight,
    gate_weight,
    query_weight,
    key_weight,
    value_weight,
    subtract_share,
    head_gain,
    output_weight,
):
    activated = jax.nn.silu(jnp.stack([condition, context_condition])).astype(jnp.bfloat16)
    partial_terms = jnp.stack(
        [
            jnp.dot(activated, matrix, preferred_element_type=jnp.float32)
            for matrix in (shift_weight, scale_weight, gate_weight)
        ]
    )
    summed = lax.psum(partial_terms, "sp")
    full_terms = lax.all_gather(summed, "tp", axis=2, tiled=True)
    shift_terms, scale_terms, gate_terms = (full_terms[0], full_terms[1], full_terms[2])
    pair_weight = jnp.concatenate([key_weight, value_weight], axis=1)
    joined = jnp.concatenate([query_weight, pair_weight], axis=1)
    projected = jnp.dot(
        modulate(
            lax.all_gather(latents, "tp", axis=0, tiled=True),
            norm_gain,
            shift_terms[0],
            scale_terms[0],
        ),
        joined,
        preferred_element_type=jnp.float32,
    )
    local_count = projected.shape[0]
    positions = lax.axis_index("sp") * local_count + jnp.arange(local_count, dtype=jnp.int32)
    cosine, sine_table = rotary_tables(positions)
    queries = rotate(projected[:, :VALUE].reshape(local_count, 2, HEAD), cosine, sine_table)
    queries = queries.reshape(local_count, VALUE).astype(jnp.bfloat16)
    latent_keys = rotate(
        projected[:, VALUE : 2 * VALUE].reshape(local_count, 2, HEAD), cosine, sine_table
    )
    latent_keys = latent_keys.reshape(local_count, VALUE).astype(jnp.bfloat16)
    latent_pairs = jnp.concatenate(
        [latent_keys, projected[:, 2 * VALUE :].astype(jnp.bfloat16)], axis=1
    )
    context_mod = modulate(context, norm_gain, shift_terms[1], scale_terms[1])
    context_pairs = jnp.dot(context_mod, pair_weight, preferred_element_type=jnp.float32).astype(
        jnp.bfloat16
    )
    sent_pairs = jnp.concatenate([latent_pairs, context_pairs], axis=0)
    arrived = lax.all_gather(sent_pairs, "sp", axis=0, tiled=True)
    updated_carry = []
    for which_map in range(2):
        offset = which_map * HEAD
        scores = jnp.einsum(
            "qd,kd->qk",
            queries[:, offset : offset + HEAD],
            arrived[:, offset : offset + HEAD],
            preferred_element_type=jnp.float32,
        ) * HEAD ** (-0.5)
        powers = jnp.exp(scores)
        updated_carry.append(
            jnp.dot(
                powers.astype(jnp.bfloat16), arrived[:, VALUE:], preferred_element_type=jnp.float32
            )
        )
        updated_carry.append(jnp.sum(powers, axis=1, keepdims=True))
    first_sum, first_total, second_sum, second_total = tuple(updated_carry)
    share_value = subtract_share[0]
    difference = first_sum / first_total - share_value * (second_sum / second_total)
    normed = difference * lax.rsqrt(
        jnp.mean(difference * difference, axis=1, keepdims=True) + head_eps
    )
    head_output = (normed * head_gain * head_scale).astype(jnp.bfloat16)
    branch = lax.psum_scatter(
        jnp.dot(head_output, output_weight, preferred_element_type=jnp.float32),
        "tp",
        scatter_dimension=0,
        tiled=True,
    )
    return (latents.astype(jnp.float32) + gate_terms[0] * branch).astype(jnp.bfloat16)


def solution(mesh):
    in_specs = (
        P(("sp", "tp"), None),
        P("sp", None),
        P("sp"),
        P("sp"),
        P(),
        P("sp", "tp"),
        P("sp", "tp"),
        P("sp", "tp"),
        P(None, "tp"),
        P(None, "tp"),
        P(None, "tp"),
        P("tp"),
        P(),
        P("tp", None),
    )
    out_specs = P(("sp", "tp"), None)
    return jax.shard_map(shards, mesh=mesh, in_specs=in_specs, out_specs=out_specs, check_vma=False)
```

profile of v0, /device:TPU:0, one launch (start us, length us, event | category | flops | bytes accessed | tf_op | source)
XLA Modules:
  0.0 143.5 jit_solution(7154837675321998949)
XLA Ops:
  6.5 0.0 copy-start
  6.5 0.0 copy-start.2
  6.5 0.0 copy-start.4
  6.5 0.0 copy-start.5
  6.5 0.0 copy-start.7
  6.5 0.0 all-gather.2.cloned.1.call-start
  6.6 0.7 all-gather.2.cloned.1.call-update
  7.3 0.0 reduce-scatter.2.cloned.1.call-start
  8.0 0.1 broadcast_multiply_fusion.1
  8.1 0.1 fusion.46
  8.2 0.1 copy.15
  8.4 0.1 copy.18
  8.5 1.1 convolution_bitcast_fusion.1
  9.6 1.1 convolution_bitcast_fusion
  10.7 0.0 copy-start.6
  10.7 1.2 convolution_bitcast_fusion.2
  11.9 8.5 %psum.7 = f32[3,2,256]{2,1,0:T(2,128)S(1)} all-reduce(f32[3,2,256]{2,1,0:T(2,128)S(1)} %pad_maximum_fusion.4), channel_id=1, replica_groups=mesh['sp'=4,'tp'=8] {'sp'}, use_global_device_ids=true, to_apply=%region_0.1 | all-reduce | flops 1536 | bytes 12288 | tf_op jit(solution)/shard_map/psum | solution.py:64
  20.4 26.4 %all_gather.9 = f32[3,2,2048]{2,1,0:T(2,128)S(1)} all-gather(f32[3,2,256]{2,1,0:T(2,128)S(1)} %psum.7), channel_id=1, replica_groups=mesh['sp'=4,'tp'=8] {'tp'}, dimensions={2}, use_global_device_ids=true | all-gather | bytes 55296 | tf_op jit(solution)/shard_map/all_gather | solution.py:65
  46.9 0.0 copy-done.2
  46.9 0.2 fusion.25
  47.1 0.0 copy-done.4
  47.1 0.0 copy-done.5
  47.1 0.0 copy-done.7
  47.1 0.3 convolution_convert_fusion
  47.5 5.4 %all-gather.2.cloned.1.call-done = bf16[256,2048]{1,0:T(8,128)(2,1)} async-done(((bf16[32,2048]{1,0:T(8,128)(2,1)}), bf16[256,2048]{1,0:T(8,128)(2,1)}) %all-gather.2.cloned.1.call-update) | async-done | bytes 1048592 | tf_op jit(solution)/shard_map/all_gather | solution.py:71
  52.9 1.5 %fusion.2 = f32[256]{0:T(256)S(1)} fusion(bf16[256,2048]{1,0:T(8,128)(2,1)} %all-gather.2.cloned.1.call-done), kind=kLoop, calls=%fused_computation.6 | loop fusion | flops 1572608 | bytes 1049600 | tf_op jit(solution)/shard_map/reduce_sum | solution.py:37
  54.4 0.0 copy-done.6
  54.4 2.0 %fusion.7 = f32[256,384]{1,0:T(8,128)S(1)} fusion(bf16[2048,128]{1,0:T(8,128)(2,1)S(1)} %copy-done.4, bf16[2048,128]{1,0:T(8,128)(2,1)S(1)} %copy-done.5, bf16[2048,128]{1,0:T(8,128)(2,1)S(1)} %copy-done.6, bf16[256,2048]{1,0:T(8,128)(2,1)} %all-gather.2.cloned.1.call-done, f32[2048]{0:T(1024)S(1)} %bitcast.40, f32[2048]{0:T(1024)S(1)} %bitcast.41, ...), kind=kOutput, calls=%fused_computation.11 | convolution fusion | flops 410517504 | bytes 3040256 | tf_op jit(solution)/shard_map/dot_general | solution.py:69
  56.5 0.1 copy.16
  56.6 0.1 copy.17
  56.7 0.1 copy.20
  56.8 0.1 copy.21
  57.0 7.9 %all_gather.11 = bf16[1280,256]{1,0:T(8,128)(2,1)S(1)} all-gather(bf16[320,256]{1,0:T(8,128)(2,1)S(1)} %pad_maximum_fusion), channel_id=1, replica_groups=mesh['sp'=4,'tp'=8] {'sp'}, dimensions={0}, use_global_device_ids=true | all-gather | bytes 819200 | tf_op jit(solution)/shard_map/all_gather | solution.py:96
  64.9 0.5 fusion.59
  65.4 0.0 copy-start.3
  65.5 0.5 fusion.60
  65.9 0.4 fusion.14
  66.3 0.4 multiply_reduce_fusion
  66.7 0.0 copy-done
  66.7 0.0 copy-done.3
  66.7 0.0 copy-start.1
  66.8 1.9 %fusion.39 = f32[256,2048]{1,0:T(8,128)} fusion(bf16[128,2048]{1,0:T(8,128)(2,1)S(1)} %copy-done, f32[256,128]{0,1:T(8,128)S(1)} %get-tuple-element.27, f32[128]{0:T(128)S(1)} %copy-done.3, f32[256]{0:T(256)S(1)} %add_rsqrt_fusion), kind=kOutput, calls=%fused_computation.58 | convolution fusion | flops 134348800 | bytes 2754048 | tf_op jit(solution)/shard_map/dot_general | solution.py:121
  68.6 0.0 reduce-scatter.2.cloned.1.call-update
  68.6 66.4 %reduce-scatter.2.cloned.1.call-done = f32[32,2048]{1,0:T(8,128)} async-done(((f32[256,2048]{1,0:T(8,128)}), f32[32,2048]{1,0:T(8,128)}) %reduce-scatter.2.cloned.1.call-update) | async-done | bytes 262160 | tf_op jit(solution)/shard_map/reduce_scatter | solution.py:120
  135.0 0.0 copy-done.1
  135.0 1.6 %add_convert_fusion = bf16[32,2048]{1,0:T(8,128)(2,1)} fusion(f32[32,2048]{1,0:T(8,128)} %reduce-scatter.2.cloned.1.call-done, bf16[32,2048]{1,0:T(8,128)(2,1)S(1)} %copy-done.1, f32[2048]{0:T(1024)S(1)} %bitcast.33), kind=kLoop, calls=%fused_computation.45 | loop fusion | flops 262144 | bytes 532480 | tf_op jit(solution)/shard_map/convert_element_type | solution.py:126
  (17 shorter events, 0.2 us)
Async XLA Ops:
  6.5 60.2 %copy-start = (bf16[128,2048]{1,0:T(8,128)(2,1)S(1)}, bf16[128,2048]{1,0:T(8,128)(2,1)}, u32[]{:S(2)}) copy-start(bf16[128,2048]{1,0:T(8,128)(2,1)} %param.27) | copy-start | bytes 1572868
  6.5 40.4 %copy-start.2 = (bf16[64,2048]{1,0:T(8,128)(2,1)S(1)}, bf16[64,2048]{1,0:T(8,128)(2,1)}, u32[]{:S(2)}) copy-start(bf16[64,2048]{1,0:T(8,128)(2,1)} %param.15) | copy-start | bytes 786436
  6.5 40.6 %copy-start.4 = (bf16[2048,128]{1,0:T(8,128)(2,1)S(1)}, bf16[2048,128]{1,0:T(8,128)(2,1)}, u32[]{:S(2)}) copy-start(bf16[2048,128]{1,0:T(8,128)(2,1)} %param.24) | copy-start | bytes 1572868
  6.5 40.6 %copy-start.5 = (bf16[2048,128]{1,0:T(8,128)(2,1)S(1)}, bf16[2048,128]{1,0:T(8,128)(2,1)}, u32[]{:S(2)}) copy-start(bf16[2048,128]{1,0:T(8,128)(2,1)} %param.23) | copy-start | bytes 1572868
  6.5 40.6 %copy-start.7 = (f32[2048]{0:T(1024)S(1)}, f32[2048]{0:T(1024)}, u32[]{:S(2)}) copy-start(f32[2048]{0:T(1024)} %param.18) | copy-start | bytes 24580
  6.5 46.3 %all-gather.2.cloned.1.call-start = ((), (), s32[]{:S(2)}) async-start(), calls=%async_computation.1 | async-start | bytes 1179648 | tf_op jit(solution)/shard_map/all_gather | solution.py:71
  7.3 127.7 %reduce-scatter.2.cloned.1.call-start = ((), (), s32[]{:S(2)}) async-start(), calls=%async_computation.2 | async-start | bytes 2359296 | tf_op jit(solution)/shard_map/reduce_scatter | solution.py:120
  10.7 43.7 %copy-start.6 = (bf16[2048,128]{1,0:T(8,128)(2,1)S(1)}, bf16[2048,128]{1,0:T(8,128)(2,1)}, u32[]{:S(2)}) copy-start(bf16[2048,128]{1,0:T(8,128)(2,1)} %param.22) | copy-start | bytes 1572868
  65.4 1.3 copy-start.3
  66.7 68.3 %copy-start.1 = (bf16[32,2048]{1,0:T(8,128)(2,1)S(1)}, bf16[32,2048]{1,0:T(8,128)(2,1)}, u32[]{:S(2)}) copy-start(bf16[32,2048]{1,0:T(8,128)(2,1)} %param.14) | copy-start | bytes 393220
Sparse Core Ops, SparseCore 0:
  9.5 43.3 all-gather.1
  68.8 66.2 reduce-scatter.1
where the time goes:
time: 144 us; the launch traced here: 143 us
  waiting for transfers between devices  72.5 us (50%)
  blocking collectives  42.9 us (30%)
  between operations  14.3 us (10%)
  matrix products  9.42 us (7%)
  other arithmetic  3.7 us (3%)
    reduce_scatter x1, waiting for transfers between devices, shards(): lax.psum_scatter(jnp.dot(head_output, output_weight, preferred_element_ty...  66.4 us
    all_gather x1, blocking collectives, shards(): full_terms = lax.all_gather(summed, 'tp', axis=2, tiled=True)  26.4 us
    psum x1, blocking collectives, shards(): summed = lax.psum(partial_terms, 'sp')  8.51 us
    all_gather x1, blocking collectives, shards(): arrived = lax.all_gather(sent_pairs, 'sp', axis=0, tiled=True)  7.9 us
    all_gather x1, waiting for transfers between devices, shards(): lax.all_gather(latents, 'tp', axis=0, tiled=True)  5.4 us
    dot_general x3, matrix products, shards(): jnp.dot(activated, matrix, preferred_element_type=jnp.float32)  3.45 us
  transfers between devices with their start and end apart: 2, of which 2 were waited for; matrix products, arithmetic and copies ran while one was open for 3% of the time, Pallas kernels for 0%

commit v1 on v0

--- a/solution.py
+++ b/solution.py
@@ -1,6 +1,11 @@
+import functools
+import math
+
 import jax
 import jax.numpy as jnp
 from jax import lax
+from jax.experimental import pallas as pl
+from jax.experimental.pallas import tpu as pltpu
 from jax.sharding import PartitionSpec as P
 
 HEAD = 64
@@ -126,6 +131,394 @@
     return (latents.astype(jnp.float32) + gate_terms[0] * branch).astype(jnp.bfloat16)
 
 
+MESH = pl.DeviceIdType.MESH
+CHUNKS = 2
+
+
+def fused_kernel(
+    lat_ref, ctx_ref, cond_ref, ccond_ref, gain_ref, shift_ref, scale_ref, gate_ref,
+    wq_hbm, wk_hbm, wv_hbm, share_ref, hgain_ref, wo_hbm, out_ref,
+    lat, mod, cmod, wqkv, wo, part, terms, tables, queries, kv, ho_send, ho,
+    load_sem, lat_ss, lat_rs, part_ss, part_rs, term_ss, term_rs,
+    kv_ss, kv_rs, ckv_ss, ckv_rs, ho_ss, ho_rs, wo_ss, wo_rs,
+    *, S, T,
+):
+    f32, bf16 = jnp.float32, jnp.bfloat16
+    rows, D = lat_ref.shape
+    crows = ctx_ref.shape[0]
+    count = rows * T
+    width = D // T
+    quarter_cols = D // S
+    Z = T // 2
+    i = lax.axis_index("sp")
+    t = lax.axis_index("tp")
+    z = lax.div(t, 2)
+    y = lax.rem(t, 2)
+    mate = t + 1 - 2 * y
+    twin = i + 1 - 2 * lax.rem(i, 2)
+    across = lax.rem(i + 2, S)
+    twin_across = lax.rem(twin + 2, S)
+    pending = []
+
+    def when(cond, action):
+        if cond is None:
+            action()
+        else:
+            pl.when(cond)(action)
+
+    def copy(src, dst, ss, rs, sp, tp):
+        return pltpu.make_async_remote_copy(
+            src_ref=src, dst_ref=dst, send_sem=ss, recv_sem=rs,
+            device_id={"sp": sp, "tp": tp}, device_id_type=MESH,
+        )
+
+    def send(cond, src, dst, ss, rs, sp, tp):
+        made = copy(src, dst, ss, rs, sp, tp)
+
+        def go():
+            made.start()
+
+        when(cond, go)
+        pending.append((cond, made))
+
+    def arrived(dst, ss, rs):
+        copy(dst, dst, ss, rs, twin, t).wait_recv()
+
+    loads = [
+        pltpu.make_async_copy(wq_hbm, wqkv.at[:, pl.ds(0, VALUE)], load_sem.at[0]),
+        pltpu.make_async_copy(wk_hbm, wqkv.at[:, pl.ds(VALUE, VALUE)], load_sem.at[1]),
+        pltpu.make_async_copy(wv_hbm, wqkv.at[:, pl.ds(2 * VALUE, VALUE)], load_sem.at[2]),
+        pltpu.make_async_copy(wo_hbm, wo.at[pl.ds(t * VALUE, VALUE), :], load_sem.at[3]),
+    ]
+    for load in loads:
+        load.start()
+
+    barrier = pltpu.get_barrier_semaphore()
+    for k in range(1, S):
+        pl.semaphore_signal(
+            barrier, inc=1, device_id={"sp": lax.rem(i + k, S), "tp": t}, device_id_type=MESH
+        )
+    for k in range(1, T):
+        pl.semaphore_signal(
+            barrier, inc=1, device_id={"sp": i, "tp": lax.rem(t + k, T)}, device_id_type=MESH
+        )
+    pl.semaphore_wait(barrier, S + T - 2)
+
+    step = rows // CHUNKS
+
+    def lat_piece(block, c):
+        return lat.at[pl.ds(block * rows + c * step, step), :]
+
+    for c in range(CHUNKS):
+        own = lat_ref.at[pl.ds(c * step, step), :]
+        dst = lat_piece(t, c)
+        rs = lat_rs.at[c, t]
+        send(z < Z - 1, own, dst, lat_ss.at[c, t, 0], rs, i, t + 2)
+        send(z > 0, own, dst, lat_ss.at[c, t, 1], rs, i, t - 2)
+        send(None, own, dst, lat_ss.at[c, t, 2], rs, i, mate)
+
+    def lat_stage(d):
+        for c in range(CHUNKS):
+            for sign in (-1, 1):
+                block = t + 2 * d * sign
+                here = z - d >= 0 if sign < 0 else z + d < Z
+                onward = jnp.logical_and(here, z < Z - 1 if sign < 0 else z > 0)
+                piece = lat_piece(block, c)
+                rs = lat_rs.at[c, block]
+
+                def come(piece=piece, rs=rs, block=block, c=c):
+                    arrived(piece, lat_ss.at[c, block, 0], rs)
+
+                when(here, come)
+                send(onward, piece, piece, lat_ss.at[c, block, 0], rs, i, t - 2 * sign)
+                send(here, piece, piece, lat_ss.at[c, block, 2], rs, i, mate)
+
+    def silu(v):
+        return v / (1.0 + jnp.exp(-v))
+
+    depth = cond_ref.shape[1]
+    line = lax.broadcasted_iota(jnp.int32, (8, depth), 0)
+    act0 = jnp.broadcast_to(silu(cond_ref[...]), (8, depth))
+    act1 = jnp.broadcast_to(silu(ccond_ref[...]), (8, depth))
+
+    def two_lines(first, matrix_ref, with_second):
+        left = jnp.where(line == first, act0, 0.0)
+        if with_second:
+            left = jnp.where(line == first + 1, act1, left)
+        return jnp.dot(left.astype(bf16), matrix_ref[...], preferred_element_type=f32)
+
+    part[pl.ds(i, 1)] = (
+        two_lines(0, shift_ref, True) + two_lines(2, scale_ref, True) + two_lines(4, gate_ref, False)
+    )[None]
+    for k in range(1, S):
+        send(None, part.at[i], part.at[i], part_ss.at[k], part_rs.at[i], lax.rem(i + k, S), t)
+
+    lat_stage(1)
+
+    for k in range(1, S):
+        peer = lax.rem(i + k, S)
+        arrived(part.at[peer], part_ss.at[k], part_rs.at[peer])
+    total = part[0]
+    for k in range(1, S):
+        total = total + part[k]
+    terms[pl.ds(t, 1)] = total[None]
+    for k in range(1, T):
+        send(None, terms.at[t], terms.at[t], term_ss.at[k], term_rs.at[t], i, lax.rem(t + k, T))
+
+    lane = lax.broadcasted_iota(jnp.int32, (count, VALUE), 1)
+    place = i * count + lax.broadcasted_iota(jnp.int32, (count, VALUE), 0)
+    spot = lax.rem(lane, HEAD)
+    quarter = HEAD // 4
+    power = lax.rem(spot, quarter).astype(f32) * (-2.0 / (HEAD // 2))
+    inverse = jnp.exp(power * math.log(rope_theta))
+    along = jnp.where(spot < HEAD // 2, lax.div(place, GRID_W), lax.rem(place, GRID_W))
+    angle = along.astype(f32) * inverse
+    even = lax.rem(lax.div(spot, quarter), 2) == 0
+    tables[0] = jnp.cos(angle)
+    tables[1] = jnp.sin(angle)
+
+    for d in range(2, Z):
+        lat_stage(d)
+
+    loads[3].wait()
+
+    def wo_piece(block, share):
+        return wo.at[pl.ds(block * VALUE, VALUE), pl.ds(share * quarter_cols, quarter_cols)]
+
+    own_wo = wo_piece(t, i)
+    send(z < Z - 1, own_wo, own_wo, wo_ss.at[t, 0], wo_rs.at[t, i], i, t + 2)
+    send(z > 0, own_wo, own_wo, wo_ss.at[t, 1], wo_rs.at[t, i], i, t - 2)
+    send(None, own_wo, own_wo, wo_ss.at[t, 2], wo_rs.at[t, i], i, mate)
+
+    def wo_side(cond, block):
+        piece = wo_piece(block, i)
+        send(cond, piece, piece, wo_ss.at[block, 3], wo_rs.at[block, i], across, t)
+        send(cond, piece, piece, wo_ss.at[block, 4], wo_rs.at[block, i], twin, t)
+
+    def wo_stage(d):
+        for sign in (-1, 1):
+            block = t + 2 * d * sign
+            here = z - d >= 0 if sign < 0 else z + d < Z
+            onward = jnp.logical_and(here, z < Z - 1 if sign < 0 else z > 0)
+            piece = wo_piece(block, i)
+            rs = wo_rs.at[block, i]
+
+            def come(piece=piece, rs=rs, block=block):
+                arrived(piece, wo_ss.at[block, 0], rs)
+
+            when(here, come)
+            send(onward, piece, piece, wo_ss.at[block, 0], rs, i, t - 2 * sign)
+            send(here, piece, piece, wo_ss.at[block, 2], rs, i, mate)
+            wo_side(here, block)
+
+    def wo_mate(d):
+        for sign in (-1, 1) if d else (1,):
+            block = mate + 2 * d * sign
+            here = None if not d else (z - d >= 0 if sign < 0 else z + d < Z)
+            piece = wo_piece(block, i)
+
+            def come(piece=piece, block=block):
+                arrived(piece, wo_ss.at[block, 0], wo_rs.at[block, i])
+
+            when(here, come)
+            wo_side(here, block)
+
+    def wo_across(column, d):
+        for sign in (-1, 1) if d else (1,):
+            block = column + 2 * d * sign
+            here = None if not d else (z - d >= 0 if sign < 0 else z + d < Z)
+            piece = wo_piece(block, across)
+
+            def come(piece=piece, block=block):
+                arrived(piece, wo_ss.at[block, 0], wo_rs.at[block, across])
+
+            when(here, come)
+            send(here, piece, piece, wo_ss.at[block, 5], wo_rs.at[block, across], twin, t)
+
+    for k in range(1, T):
+        peer = lax.rem(t + k, T)
+        arrived(terms.at[peer], term_ss.at[k], term_rs.at[peer])
+
+    def modulate_into(dst, src, first, n, which):
+        wide = src[...].astype(f32)
+        factor = lax.rsqrt(jnp.mean(wide * wide, axis=-1, keepdims=True) + norm_eps)
+        for j in range(T):
+            cols = slice(j * width, (j + 1) * width)
+            mult = gain_ref[:, cols] * (1.0 + terms[j, 2 + which : 3 + which, :])
+            shifted = wide[:, cols] * factor * mult + terms[j, which : which + 1, :]
+            dst[pl.ds(first, n), cols] = shifted.astype(bf16)
+
+    for load in loads[:3]:
+        load.wait()
+    modulate_into(cmod, ctx_ref, 0, crows, 1)
+    kv[pl.ds(i, 1), pl.ds(count, crows), :] = jnp.dot(
+        cmod[...], wqkv[:, VALUE:], preferred_element_type=f32
+    ).astype(bf16)[None]
+
+    def ckv_piece(s):
+        return kv.at[s, pl.ds(count, crows), :]
+
+    def kv_piece(s):
+        return kv.at[s, pl.ds(0, count), :]
+
+    send(None, ckv_piece(i), ckv_piece(i), ckv_ss.at[0], ckv_rs.at[i], across, t)
+    send(None, ckv_piece(i), ckv_piece(i), ckv_ss.at[1], ckv_rs.at[i], twin, t)
+
+    for d in range(Z):
+        for sign in (-1, 1) if d else (1,):
+            block = mate + 2 * d * sign
+            here = None if not d else (z - d >= 0 if sign < 0 else z + d < Z)
+            for c in range(CHUNKS):
+                def come(block=block, c=c):
+                    arrived(lat_piece(block, c), lat_ss.at[c, block, 0], lat_rs.at[c, block])
+
+                when(here, come)
+    lat[pl.ds(t * rows, rows), :] = lat_ref[...]
+    modulate_into(mod, lat, 0, count, 0)
+    projected = jnp.dot(mod[...], wqkv[...], preferred_element_type=f32)
+
+    def rotated(u):
+        turned = jnp.where(even, -pltpu.roll(u, VALUE - quarter, 1), pltpu.roll(u, quarter, 1))
+        return u * tables[0] + turned * tables[1]
+
+    kv[pl.ds(i, 1), pl.ds(0, count), pl.ds(0, VALUE)] = (
+        rotated(projected[:, VALUE : 2 * VALUE]).astype(bf16)[None]
+    )
+    kv[pl.ds(i, 1), pl.ds(0, count), pl.ds(VALUE, VALUE)] = (
+        projected[:, 2 * VALUE :].astype(bf16)[None]
+    )
+    send(None, kv_piece(i), kv_piece(i), kv_ss.at[0], kv_rs.at[i], across, t)
+    send(None, kv_piece(i), kv_piece(i), kv_ss.at[1], kv_rs.at[i], twin, t)
+    arrived(ckv_piece(across), ckv_ss.at[2], ckv_rs.at[across])
+    send(None, ckv_piece(across), ckv_piece(across), ckv_ss.at[2], ckv_rs.at[across], twin, t)
+    query = rotated(projected[:, :VALUE]).astype(bf16) * jnp.asarray(HEAD ** (-0.5), bf16)
+    first_half = lane < HEAD
+    zero = jnp.zeros_like(query)
+    queries[0:count, :] = jnp.where(first_half, query, zero)
+    queries[count:, :] = jnp.where(first_half, zero, query)
+    wo_stage(1)
+    wo_mate(0)
+
+    ones = jnp.ones((count + crows, VALUE), bf16)
+
+    def attend(slot):
+        rows_kv = kv[slot]
+        scores = lax.dot_general(
+            queries[...], rows_kv[:, :VALUE], (((1,), (1,)), ((), ())), preferred_element_type=f32
+        )
+        return jnp.dot(
+            jnp.exp(scores).astype(bf16),
+            jnp.concatenate([rows_kv[:, VALUE:], ones], axis=1),
+            preferred_element_type=f32,
+        )
+
+    sums = attend(i)
+    wo_stage(2) if Z > 2 else None
+    arrived(kv_piece(twin), kv_ss.at[2], kv_rs.at[twin])
+    arrived(ckv_piece(twin), ckv_ss.at[2], ckv_rs.at[twin])
+    sums = sums + attend(twin)
+    wo_mate(1)
+    arrived(kv_piece(across), kv_ss.at[2], kv_rs.at[across])
+    send(None, kv_piece(across), kv_piece(across), kv_ss.at[2], kv_rs.at[across], twin, t)
+    sums = sums + attend(across)
+    arrived(kv_piece(twin_across), kv_ss.at[2], kv_rs.at[twin_across])
+    arrived(ckv_piece(twin_across), ckv_ss.at[2], ckv_rs.at[twin_across])
+    sums = sums + attend(twin_across)
+    ratio = sums[:, :VALUE] / sums[:, VALUE:]
+    difference = ratio[:count] - share_ref[0] * ratio[count:]
+    normed = difference * lax.rsqrt(
+        jnp.mean(difference * difference, axis=1, keepdims=True) + head_eps
+    )
+    ho_send[...] = (normed * hgain_ref[...] * head_scale).astype(bf16)
+    for k in range(1, T):
+        peer = lax.rem(t + k, T)
+        send(
+            None, ho_send.at[pl.ds(peer * rows, rows), :], ho.at[t], ho_ss.at[k], ho_rs.at[t], i, peer
+        )
+    ho[pl.ds(t, 1)] = ho_send[pl.ds(t * rows, rows), :][None]
+
+    for d in range(3, Z):
+        wo_stage(d)
+    for d in range(2, Z):
+        wo_mate(d)
+    for d in range(Z):
+        if d:
+            wo_across(t, d)
+        wo_across(mate, d)
+    for k in range(1, T):
+        peer = lax.rem(t + k, T)
+        arrived(ho.at[peer], ho_ss.at[k], ho_rs.at[peer])
+        for share in (twin, twin_across):
+            arrived(wo_piece(peer, share), wo_ss.at[peer, 0], wo_rs.at[peer, share])
+    heads = jnp.concatenate([ho[h] for h in range(T)], axis=1)
+    for j in range(T):
+        cols = slice(j * width, (j + 1) * width)
+        branch = jnp.dot(heads, wo[:, cols], preferred_element_type=f32)
+        out_ref[:, cols] = (
+            lat_ref[:, cols].astype(f32) + terms[j, 4:5, :] * branch
+        ).astype(bf16)
+
+    for cond, made in pending:
+        def finish(made=made):
+            made.wait_send()
+
+        when(cond, finish)
+
+
+def fused_shards(S, T, *args):
+    (latents, context, condition, context_condition, norm_gain, shift_weight, scale_weight,
+     gate_weight, query_weight, key_weight, value_weight, subtract_share, head_gain,
+     output_weight) = args
+    rows, D = latents.shape
+    crows = context.shape[0]
+    count = rows * T
+    bf16, f32 = jnp.bfloat16, jnp.float32
+    vmem = pl.BlockSpec(memory_space=pltpu.VMEM)
+    hbm = pl.BlockSpec(memory_space=pl.ANY)
+    smem = pl.BlockSpec(memory_space=pltpu.SMEM)
+    dma = pltpu.SemaphoreType.DMA
+    return pl.pallas_call(
+        functools.partial(fused_kernel, S=S, T=T),
+        out_shape=jax.ShapeDtypeStruct((rows, D), bf16),
+        in_specs=[vmem] * 8 + [hbm] * 3 + [smem, vmem, hbm],
+        out_specs=vmem,
+        scratch_shapes=[
+            pltpu.VMEM((count, D), bf16),
+            pltpu.VMEM((count, D), bf16),
+            pltpu.VMEM((crows, D), bf16),
+            pltpu.VMEM((D, 3 * VALUE), bf16),
+            pltpu.VMEM((T * VALUE, D), bf16),
+            pltpu.VMEM((S, 8, D // T), f32),
+            pltpu.VMEM((T, 8, D // T), f32),
+            pltpu.VMEM((2, count, VALUE), f32),
+            pltpu.VMEM((2 * count, VALUE), bf16),
+            pltpu.VMEM((S, count + crows, 2 * VALUE), bf16),
+            pltpu.VMEM((count, VALUE), bf16),
+            pltpu.VMEM((T, rows, VALUE), bf16),
+            dma((4,)), dma((CHUNKS, T, 3)), dma((CHUNKS, T)), dma((S,)), dma((S,)),
+            dma((T,)), dma((T,)), dma((3,)), dma((S,)), dma((3,)), dma((S,)),
+            dma((T,)), dma((T,)), dma((T, 6)), dma((T, S)),
+        ],
+        compiler_params=pltpu.CompilerParams(
+            collective_id=0, has_side_effects=True, vmem_limit_bytes=56 * 1024 * 1024
+        ),
+    )(latents, context, condition[None, :], context_condition[None, :], norm_gain[None, :],
+      shift_weight, scale_weight, gate_weight, query_weight, key_weight, value_weight,
+      subtract_share, head_gain[None, :], output_weight)
+
+
+def fits(S, T, shapes):
+    rows = shapes[0][0] // (S * T)
+    crows = shapes[1][0] // S
+    D = shapes[0][1]
+    heads = shapes[8][1] // VALUE
+    return (
+        S == 4 and T % 2 == 0 and heads == T and rows % (16 * CHUNKS) == 0
+        and crows % 16 == 0 and D % (128 * T) == 0 and T >= 4
+        and rows * T * D * 8 + T * VALUE * D * 2 < 24 * 1024 * 1024
+    )
+
+
 def solution(mesh):
     in_specs = (
         P(("sp", "tp"), None),
@@ -144,4 +537,15 @@
         P("tp", None),
     )
     out_specs = P(("sp", "tp"), None)
-    return jax.shard_map(shards, mesh=mesh, in_specs=in_specs, out_specs=out_specs, check_vma=False)
+    S, T = mesh.shape["sp"], mesh.shape["tp"]
+
+    def whole(*args):
+        if fits(S, T, [a.shape for a in args]):
+            body = functools.partial(fused_shards, S, T)
+        else:
+            body = shards
+        return jax.shard_map(
+            body, mesh=mesh, in_specs=in_specs, out_specs=out_specs, check_vma=False
+        )(*args)
+
+    return whole

time: 144 us -> 52.2 us (0.36)
  waiting for transfers between devices: 72.5 us -> 0 us
  Pallas kernels: 0 us -> 49 us
  blocking collectives: 42.9 us -> 0 us
  between operations: 14.3 us -> 0.66 us
  matrix products: 9.42 us -> 0 us
  other arithmetic: 3.7 us -> 0 us
    reduce_scatter x1 -> x0, waiting for transfers between devices: 66.4 us -> none  [shards(): lax.psum_scatter(jnp.dot(head_output, output_weight, preferred_element_ty...]
    pallas_call x0 -> x1, Pallas kernels: none -> 49 us  [fused_shards(): pl.pallas_call(functools.partial(fused_kernel, S=S, T=T), out_shape=jax.S...]
    all_gather x2 -> x0, blocking collectives: 34.3 us -> none  [the longest x1 26.4 us: shards(): full_terms = lax.all_gather(summed, 'tp', axis=2, tiled=True)]
    dot_general x10 -> x0, matrix products: 9.42 us -> none  [the longest x3 3.45 us: shards(): jnp.dot(activated, matrix, preferred_element_type=jnp.float32)]
    psum x1 -> x0, blocking collectives: 8.51 us -> none  [shards(): summed = lax.psum(partial_terms, 'sp')]
    all_gather x1 -> x0, waiting for transfers between devices: 5.4 us -> none  [shards(): lax.all_gather(latents, 'tp', axis=0, tiled=True)]
    convert_element_type x3 -> x0, other arithmetic: 1.69 us -> none  [the longest x1 1.64 us: shards(): (latents.astype(jnp.float32) + gate_terms[0] * branch).astype(jnp.bfloat16)]
    reduce_sum x2 -> x0, other arithmetic: 1.66 us -> none  [modulate(): jnp.mean(widened * widened, axis=-1, keepdims=True) + norm_eps]
  transfers between devices with their start and end apart: 2 -> 0, of which waited for: 2 -> 0; matrix products, arithmetic and copies ran while one was open for 3% -> 0% of each run, Pallas kernels for 0% -> 0%
where the time goes in v1:
time: 52.2 us; the launch traced here: 51.2 us
  Pallas kernels  49 us (94%)
  local copies, waits for them, and re-layouts  1.57 us (3%)
  between operations  0.66 us (1%)
    pallas_call x1, Pallas kernels, fused_shards(): pl.pallas_call(functools.partial(fused_kernel, S=S, T=T), out_shape=jax.S...  49 us
    unnamed x1, local copies, waits for them, and re-layouts  1.57 us

profile of v1, /device:TPU:0, one launch (start us, length us, event | category | flops | bytes accessed | tf_op | source)
XLA Modules:
  0.0 51.2 jit_solution(14174059412646876204)
XLA Ops:
  0.7 49.0 %shard_map.136 = bf16[32,2048]{1,0:T(8,128)(2,1)} custom-call(bf16[32,2048]{1,0:T(8,128)(2,1)} %lat_ref.1, bf16[64,2048]{1,0:T(8,128)(2,1)} %ctx_ref.1, f32[1,512]{1,0:T(1,128)} %bitcast.5, f32[1,512]{1,0:T(1,128)} %bitcast.6, f32[1,2048]{1,0:T(1,128)} %bitcast.4, bf16[512,256]{1,0:T(8,128)(2,1)} %shift_ref.1, bf16[512,256]{1,0:T(8,128)(2,1)} %scale_ref.1, ...), custom_call_target="tpu_custom_call" | custom-call | tf_op jit(solution)/shard_map/pallas_call | solution.py:480
  49.7 1.6 %copy.17 = bf16[32,2048]{1,0:T(8,128)(2,1)} copy(bf16[32,2048]{1,0:T(8,128)(2,1)} %shard_map.136) | data formatting | bytes 262144

commit v2 on v1

--- a/solution.py
+++ b/solution.py
@@ -133,14 +133,16 @@
 
 MESH = pl.DeviceIdType.MESH
 CHUNKS = 2
+FAR_PIECES = 2
 
 
 def fused_kernel(
-    lat_ref, ctx_ref, cond_ref, ccond_ref, gain_ref, shift_ref, scale_ref, gate_ref,
+    lat_ref, ctx_ref, cond_ref, ccond_ref, gain_ref, shift_hbm, scale_hbm, gate_hbm,
     wq_hbm, wk_hbm, wv_hbm, share_ref, hgain_ref, wo_hbm, out_ref,
     lat, mod, cmod, wqkv, wo, part, terms, tables, queries, kv, ho_send, ho,
+    shift_ref, scale_ref, gate_ref, far_send, far_recv,
     load_sem, lat_ss, lat_rs, part_ss, part_rs, term_ss, term_rs,
-    kv_ss, kv_rs, ckv_ss, ckv_rs, ho_ss, ho_rs, wo_ss, wo_rs,
+    kv_ss, kv_rs, ckv_ss, ckv_rs, ho_ss, ho_rs, hx_ss, hx_rs, wo_ss, wo_rs, far_ss, far_rs,
     *, S, T,
 ):
     f32, bf16 = jnp.float32, jnp.bfloat16
@@ -158,6 +160,9 @@
     twin = i + 1 - 2 * lax.rem(i, 2)
     across = lax.rem(i + 2, S)
     twin_across = lax.rem(twin + 2, S)
+    core = lax.rem(i, 2)
+    side = lax.div(i, 2)
+    half = D // 2
     pending = []
 
     def when(cond, action):
@@ -188,10 +193,15 @@
         pltpu.make_async_copy(wq_hbm, wqkv.at[:, pl.ds(0, VALUE)], load_sem.at[0]),
         pltpu.make_async_copy(wk_hbm, wqkv.at[:, pl.ds(VALUE, VALUE)], load_sem.at[1]),
         pltpu.make_async_copy(wv_hbm, wqkv.at[:, pl.ds(2 * VALUE, VALUE)], load_sem.at[2]),
-        pltpu.make_async_copy(wo_hbm, wo.at[pl.ds(t * VALUE, VALUE), :], load_sem.at[3]),
+        pltpu.make_async_copy(
+            wo_hbm.at[:, pl.ds(pl.multiple_of(side * half, half), half)],
+            wo.at[pl.ds(t * VALUE, VALUE), :],
+            load_sem.at[3],
+        ),
+        pltpu.make_async_copy(shift_hbm, shift_ref, load_sem.at[4]),
+        pltpu.make_async_copy(scale_hbm, scale_ref, load_sem.at[5]),
+        pltpu.make_async_copy(gate_hbm, gate_ref, load_sem.at[6]),
     ]
-    for load in loads:
-        load.start()
 
     barrier = pltpu.get_barrier_semaphore()
     for k in range(1, S):
@@ -202,7 +212,12 @@
         pl.semaphore_signal(
             barrier, inc=1, device_id={"sp": i, "tp": lax.rem(t + k, T)}, device_id_type=MESH
         )
-    pl.semaphore_wait(barrier, S + T - 2)
+        pl.semaphore_signal(
+            barrier, inc=1, device_id={"sp": across, "tp": lax.rem(t + k, T)}, device_id_type=MESH
+        )
+    for load in loads[4:] + loads[:4]:
+        load.start()
+    pl.semaphore_wait(barrier, S + 2 * T - 3)
 
     step = rows // CHUNKS
 
@@ -247,6 +262,8 @@
             left = jnp.where(line == first + 1, act1, left)
         return jnp.dot(left.astype(bf16), matrix_ref[...], preferred_element_type=f32)
 
+    for load in loads[4:]:
+        load.wait()
     part[pl.ds(i, 1)] = (
         two_lines(0, shift_ref, True) + two_lines(2, scale_ref, True) + two_lines(4, gate_ref, False)
     )[None]
@@ -277,31 +294,23 @@
     tables[0] = jnp.cos(angle)
     tables[1] = jnp.sin(angle)
 
-    for d in range(2, Z):
-        lat_stage(d)
-
-    loads[3].wait()
-
     def wo_piece(block, share):
-        return wo.at[pl.ds(block * VALUE, VALUE), pl.ds(share * quarter_cols, quarter_cols)]
-
-    own_wo = wo_piece(t, i)
-    send(z < Z - 1, own_wo, own_wo, wo_ss.at[t, 0], wo_rs.at[t, i], i, t + 2)
-    send(z > 0, own_wo, own_wo, wo_ss.at[t, 1], wo_rs.at[t, i], i, t - 2)
-    send(None, own_wo, own_wo, wo_ss.at[t, 2], wo_rs.at[t, i], i, mate)
-
-    def wo_side(cond, block):
-        piece = wo_piece(block, i)
-        send(cond, piece, piece, wo_ss.at[block, 3], wo_rs.at[block, i], across, t)
-        send(cond, piece, piece, wo_ss.at[block, 4], wo_rs.at[block, i], twin, t)
+        return wo.at[
+            pl.ds(block * VALUE, VALUE),
+            pl.ds(pl.multiple_of(share * quarter_cols, quarter_cols), quarter_cols),
+        ]
+
+    def wo_twin(cond, block):
+        piece = wo_piece(block, core)
+        send(cond, piece, piece, wo_ss.at[block, 3], wo_rs.at[block, core], twin, t)
 
     def wo_stage(d):
         for sign in (-1, 1):
             block = t + 2 * d * sign
             here = z - d >= 0 if sign < 0 else z + d < Z
             onward = jnp.logical_and(here, z < Z - 1 if sign < 0 else z > 0)
-            piece = wo_piece(block, i)
-            rs = wo_rs.at[block, i]
+            piece = wo_piece(block, core)
+            rs = wo_rs.at[block, core]
 
             def come(piece=piece, rs=rs, block=block):
                 arrived(piece, wo_ss.at[block, 0], rs)
@@ -309,31 +318,28 @@
             when(here, come)
             send(onward, piece, piece, wo_ss.at[block, 0], rs, i, t - 2 * sign)
             send(here, piece, piece, wo_ss.at[block, 2], rs, i, mate)
-            wo_side(here, block)
+            wo_twin(here, block)
 
     def wo_mate(d):
         for sign in (-1, 1) if d else (1,):
             block = mate + 2 * d * sign
             here = None if not d else (z - d >= 0 if sign < 0 else z + d < Z)
-            piece = wo_piece(block, i)
+            piece = wo_piece(block, core)
 
             def come(piece=piece, block=block):
-                arrived(piece, wo_ss.at[block, 0], wo_rs.at[block, i])
+                arrived(piece, wo_ss.at[block, 0], wo_rs.at[block, core])
 
             when(here, come)
-            wo_side(here, block)
-
-    def wo_across(column, d):
-        for sign in (-1, 1) if d else (1,):
-            block = column + 2 * d * sign
-            here = None if not d else (z - d >= 0 if sign < 0 else z + d < Z)
-            piece = wo_piece(block, across)
-
-            def come(piece=piece, block=block):
-                arrived(piece, wo_ss.at[block, 0], wo_rs.at[block, across])
-
-            when(here, come)
-            send(here, piece, piece, wo_ss.at[block, 5], wo_rs.at[block, across], twin, t)
+            wo_twin(here, block)
+
+    loads[3].wait()
+    own_wo = wo_piece(t, core)
+    for d in range(2, Z):
+        lat_stage(d)
+        if d == 2:
+            send(z < Z - 1, own_wo, own_wo, wo_ss.at[t, 0], wo_rs.at[t, core], i, t + 2)
+            send(z > 0, own_wo, own_wo, wo_ss.at[t, 1], wo_rs.at[t, core], i, t - 2)
+    send(None, own_wo, own_wo, wo_ss.at[t, 2], wo_rs.at[t, core], i, mate)
 
     for k in range(1, T):
         peer = lax.rem(t + k, T)
@@ -389,6 +395,7 @@
     )
     send(None, kv_piece(i), kv_piece(i), kv_ss.at[0], kv_rs.at[i], across, t)
     send(None, kv_piece(i), kv_piece(i), kv_ss.at[1], kv_rs.at[i], twin, t)
+    wo_stage(1)
     arrived(ckv_piece(across), ckv_ss.at[2], ckv_rs.at[across])
     send(None, ckv_piece(across), ckv_piece(across), ckv_ss.at[2], ckv_rs.at[across], twin, t)
     query = rotated(projected[:, :VALUE]).astype(bf16) * jnp.asarray(HEAD ** (-0.5), bf16)
@@ -396,8 +403,6 @@
     zero = jnp.zeros_like(query)
     queries[0:count, :] = jnp.where(first_half, query, zero)
     queries[count:, :] = jnp.where(first_half, zero, query)
-    wo_stage(1)
-    wo_mate(0)
 
     ones = jnp.ones((count + crows, VALUE), bf16)
 
@@ -413,14 +418,15 @@
         )
 
     sums = attend(i)
-    wo_stage(2) if Z > 2 else None
     arrived(kv_piece(twin), kv_ss.at[2], kv_rs.at[twin])
     arrived(ckv_piece(twin), ckv_ss.at[2], ckv_rs.at[twin])
     sums = sums + attend(twin)
-    wo_mate(1)
+    wo_mate(0)
+    wo_stage(2)
     arrived(kv_piece(across), kv_ss.at[2], kv_rs.at[across])
     send(None, kv_piece(across), kv_piece(across), kv_ss.at[2], kv_rs.at[across], twin, t)
     sums = sums + attend(across)
+    wo_mate(1)
     arrived(kv_piece(twin_across), kv_ss.at[2], kv_rs.at[twin_across])
     arrived(ckv_piece(twin_across), ckv_ss.at[2], ckv_rs.at[twin_across])
     sums = sums + attend(twin_across)
@@ -433,30 +439,55 @@
     for k in range(1, T):
         peer = lax.rem(t + k, T)
         send(
-            None, ho_send.at[pl.ds(peer * rows, rows), :], ho.at[t], ho_ss.at[k], ho_rs.at[t], i, peer
-        )
-    ho[pl.ds(t, 1)] = ho_send[pl.ds(t * rows, rows), :][None]
+            None, ho_send.at[pl.ds(peer * rows, rows), :], ho.at[0, t], ho_ss.at[k], ho_rs.at[t], i, peer
+        )
+    for k in range(T):
+        peer = lax.rem(t + k, T)
+        send(
+            None, ho_send.at[pl.ds(peer * rows, rows), :], ho.at[1, t], hx_ss.at[k], hx_rs.at[t], across, peer
+        )
+    ho[0, pl.ds(t, 1)] = ho_send[pl.ds(t * rows, rows), :][None]
 
     for d in range(3, Z):
         wo_stage(d)
     for d in range(2, Z):
         wo_mate(d)
-    for d in range(Z):
-        if d:
-            wo_across(t, d)
-        wo_across(mate, d)
-    for k in range(1, T):
+    for k in range(T):
         peer = lax.rem(t + k, T)
-        arrived(ho.at[peer], ho_ss.at[k], ho_rs.at[peer])
-        for share in (twin, twin_across):
-            arrived(wo_piece(peer, share), wo_ss.at[peer, 0], wo_rs.at[peer, share])
-    heads = jnp.concatenate([ho[h] for h in range(T)], axis=1)
-    for j in range(T):
-        cols = slice(j * width, (j + 1) * width)
-        branch = jnp.dot(heads, wo[:, cols], preferred_element_type=f32)
-        out_ref[:, cols] = (
-            lat_ref[:, cols].astype(f32) + terms[j, 4:5, :] * branch
-        ).astype(bf16)
+        if k:
+            arrived(wo_piece(peer, 1 - core), wo_ss.at[peer, 0], wo_rs.at[peer, 1 - core])
+            arrived(ho.at[0, peer], ho_ss.at[k], ho_rs.at[peer])
+        arrived(ho.at[1, peer], hx_ss.at[k], hx_rs.at[peer])
+    heads = jnp.concatenate(
+        [jnp.concatenate([ho[which, h] for h in range(T)], axis=1) for which in (1, 0)], axis=0
+    )
+    near = []
+    blocks = T // 2
+    per_piece = blocks // FAR_PIECES
+    for j in range(blocks):
+        gated = terms[pl.ds(side * blocks + j, 1), 4:5, :][0] * jnp.dot(
+            heads, wo[:, j * width : (j + 1) * width], preferred_element_type=f32
+        )
+        far_send[:, j * width : (j + 1) * width] = gated[:rows].astype(bf16)
+        near.append(gated[rows:])
+        if (j + 1) % per_piece == 0:
+            n = j // per_piece
+            piece = pl.ds(n * per_piece * width, per_piece * width)
+            send(
+                None, far_send.at[:, piece], far_recv.at[:, piece], far_ss.at[n], far_rs.at[n], across, t
+            )
+    for j in range(blocks):
+        cols = pl.ds(pl.multiple_of(side * half + j * width, width), width)
+        out_ref[:, cols] = (lat_ref[:, cols].astype(f32) + near[j]).astype(bf16)
+    for n in range(FAR_PIECES):
+        piece = pl.ds(n * per_piece * width, per_piece * width)
+        arrived(far_recv.at[:, piece], far_ss.at[n], far_rs.at[n])
+        for j in range(n * per_piece, (n + 1) * per_piece):
+            cols = pl.ds(pl.multiple_of((1 - side) * half + j * width, width), width)
+            out_ref[:, cols] = (
+                lat_ref[:, cols].astype(f32)
+                + far_recv[:, j * width : (j + 1) * width].astype(f32)
+            ).astype(bf16)
 
     for cond, made in pending:
         def finish(made=made):
@@ -480,24 +511,30 @@
     return pl.pallas_call(
         functools.partial(fused_kernel, S=S, T=T),
         out_shape=jax.ShapeDtypeStruct((rows, D), bf16),
-        in_specs=[vmem] * 8 + [hbm] * 3 + [smem, vmem, hbm],
+        in_specs=[vmem] * 5 + [hbm] * 6 + [smem, vmem, hbm],
         out_specs=vmem,
         scratch_shapes=[
             pltpu.VMEM((count, D), bf16),
             pltpu.VMEM((count, D), bf16),
             pltpu.VMEM((crows, D), bf16),
             pltpu.VMEM((D, 3 * VALUE), bf16),
-            pltpu.VMEM((T * VALUE, D), bf16),
+            pltpu.VMEM((T * VALUE, D // 2), bf16),
             pltpu.VMEM((S, 8, D // T), f32),
             pltpu.VMEM((T, 8, D // T), f32),
             pltpu.VMEM((2, count, VALUE), f32),
             pltpu.VMEM((2 * count, VALUE), bf16),
             pltpu.VMEM((S, count + crows, 2 * VALUE), bf16),
             pltpu.VMEM((count, VALUE), bf16),
-            pltpu.VMEM((T, rows, VALUE), bf16),
-            dma((4,)), dma((CHUNKS, T, 3)), dma((CHUNKS, T)), dma((S,)), dma((S,)),
+            pltpu.VMEM((2, T, rows, VALUE), bf16),
+            pltpu.VMEM(shift_weight.shape, bf16),
+            pltpu.VMEM(shift_weight.shape, bf16),
+            pltpu.VMEM(shift_weight.shape, bf16),
+            pltpu.VMEM((rows, D // 2), bf16),
+            pltpu.VMEM((rows, D // 2), bf16),
+            dma((7,)), dma((CHUNKS, T, 3)), dma((CHUNKS, T)), dma((S,)), dma((S,)),
             dma((T,)), dma((T,)), dma((3,)), dma((S,)), dma((3,)), dma((S,)),
-            dma((T,)), dma((T,)), dma((T, 6)), dma((T, S)),
+            dma((T,)), dma((T,)), dma((T,)), dma((T,)), dma((T, 4)), dma((T, 2)),
+            dma((FAR_PIECES,)), dma((FAR_PIECES,)),
         ],
         compiler_params=pltpu.CompilerParams(
             collective_id=0, has_side_effects=True, vmem_limit_bytes=56 * 1024 * 1024
@@ -513,8 +550,8 @@
     D = shapes[0][1]
     heads = shapes[8][1] // VALUE
     return (
-        S == 4 and T % 2 == 0 and heads == T and rows % (16 * CHUNKS) == 0
-        and crows % 16 == 0 and D % (128 * T) == 0 and T >= 4
+        S == 4 and T % (2 * FAR_PIECES) == 0 and heads == T and rows % (16 * CHUNKS) == 0
+        and crows % 16 == 0 and D % (128 * T) == 0 and T >= 8
         and rows * T * D * 8 + T * VALUE * D * 2 < 24 * 1024 * 1024
     )
 

time: 52.2 us -> 47 us (0.900); the launches traced: 51.2 us -> 46.8 us
  Pallas kernels: 49 us -> 44.6 us
    pallas_call x1, Pallas kernels: 49 us -> 44.6 us  [fused_shards(): pl.pallas_call(functools.partial(fused_kernel, S=S, T=T), out_shape=jax.S...]
where the time goes in v2:
time: 47 us; the launch traced here: 46.8 us
  Pallas kernels  44.6 us (95%)
  local copies, waits for them, and re-layouts  1.57 us (3%)
  between operations  0.66 us (1%)
    pallas_call x1, Pallas kernels, fused_shards(): pl.pallas_call(functools.partial(fused_kernel, S=S, T=T), out_shape=jax.S...  44.6 us
    unnamed x1, local copies, waits for them, and re-layouts  1.57 us

profile of v2, /device:TPU:0, one launch (start us, length us, event | category | flops | bytes accessed | tf_op | source)
XLA Modules:
  0.0 46.8 jit_solution(3806887958513336466)
XLA Ops:
  0.7 44.6 %shard_map.136 = bf16[32,2048]{1,0:T(8,128)(2,1)} custom-call(bf16[32,2048]{1,0:T(8,128)(2,1)} %lat_ref.1, bf16[64,2048]{1,0:T(8,128)(2,1)} %ctx_ref.1, f32[1,512]{1,0:T(1,128)} %bitcast.5, f32[1,512]{1,0:T(1,128)} %bitcast.6, f32[1,2048]{1,0:T(1,128)} %bitcast.4, bf16[512,256]{1,0:T(8,128)(2,1)} %shift_hbm.1, bf16[512,256]{1,0:T(8,128)(2,1)} %scale_hbm.1, ...), custom_call_target="tpu_custom_call" | custom-call | tf_op jit(solution)/shard_map/pallas_call | solution.py:511
  45.2 1.6 %copy.17 = bf16[32,2048]{1,0:T(8,128)(2,1)} copy(bf16[32,2048]{1,0:T(8,128)(2,1)} %shard_map.136) | data formatting | bytes 262144

commit v3 on v2

--- a/solution.py
+++ b/solution.py
@@ -132,7 +132,8 @@
 
 
 MESH = pl.DeviceIdType.MESH
-CHUNKS = 2
+CHUNKS = 4
+WEIGHT_CHUNKS = 2
 FAR_PIECES = 2
 
 
@@ -141,8 +142,8 @@
     wq_hbm, wk_hbm, wv_hbm, share_ref, hgain_ref, wo_hbm, out_ref,
     lat, mod, cmod, wqkv, wo, part, terms, tables, queries, kv, ho_send, ho,
     shift_ref, scale_ref, gate_ref, far_send, far_recv,
-    load_sem, lat_ss, lat_rs, part_ss, part_rs, term_ss, term_rs,
-    kv_ss, kv_rs, ckv_ss, ckv_rs, ho_ss, ho_rs, hx_ss, hx_rs, wo_ss, wo_rs, far_ss, far_rs,
+    load_sem, lat_ss, lat_rs, lat_yss, lat_yrs, part_ss, part_rs, term_ss, term_rs,
+    kv_ss, kv_rs, ckv_ss, ckv_rs, ho_ss, ho_rs, hx_ss, hx_rs, wo_ss, wo_rs, wo_mrs, wo_yss, wo_tss, wo_trs, far_ss, far_rs,
     *, S, T,
 ):
     f32, bf16 = jnp.float32, jnp.bfloat16
@@ -157,6 +158,8 @@
     z = lax.div(t, 2)
     y = lax.rem(t, 2)
     mate = t + 1 - 2 * y
+    even_layer = lax.rem(z, 2) == 0
+    paired = t + 2 - 4 * lax.rem(z, 2)
     twin = i + 1 - 2 * lax.rem(i, 2)
     across = lax.rem(i + 2, S)
     twin_across = lax.rem(twin + 2, S)
@@ -164,6 +167,7 @@
     side = lax.div(i, 2)
     half = D // 2
     pending = []
+    late = []
 
     def when(cond, action):
         if cond is None:
@@ -177,14 +181,26 @@
             device_id={"sp": sp, "tp": tp}, device_id_type=MESH,
         )
 
-    def send(cond, src, dst, ss, rs, sp, tp):
+    def send(cond, src, dst, ss, rs, sp, tp, tracked=True):
         made = copy(src, dst, ss, rs, sp, tp)
 
         def go():
             made.start()
 
         when(cond, go)
-        pending.append((cond, made))
+        if tracked:
+            pending.append((cond, made))
+
+    def drain():
+        for cond, made in pending:
+            def finish(made=made):
+                made.wait_send()
+
+            when(cond, finish)
+        pending.clear()
+
+    def sent_all(view, ss):
+        copy(view, view, ss, ss, twin, t).wait_send()
 
     def arrived(dst, ss, rs):
         copy(dst, dst, ss, rs, twin, t).wait_recv()
@@ -219,18 +235,18 @@
         load.start()
     pl.semaphore_wait(barrier, S + 2 * T - 3)
 
-    step = rows // CHUNKS
+    step = D // CHUNKS
 
     def lat_piece(block, c):
-        return lat.at[pl.ds(block * rows + c * step, step), :]
+        return lat.at[pl.ds(block * rows, rows), pl.ds(c * step, step)]
 
     for c in range(CHUNKS):
-        own = lat_ref.at[pl.ds(c * step, step), :]
+        own = lat_ref.at[:, pl.ds(c * step, step)]
         dst = lat_piece(t, c)
-        rs = lat_rs.at[c, t]
-        send(z < Z - 1, own, dst, lat_ss.at[c, t, 0], rs, i, t + 2)
-        send(z > 0, own, dst, lat_ss.at[c, t, 1], rs, i, t - 2)
-        send(None, own, dst, lat_ss.at[c, t, 2], rs, i, mate)
+        send(z < Z - 1, own, dst, lat_ss.at[c, z], lat_rs.at[c, z], i, t + 2)
+        send(z > 0, own, dst, lat_ss.at[c, Z], lat_rs.at[c, z], i, t - 2)
+        rs = lat_rs.at[c, Z] if c >= CHUNKS // 2 else lat_yrs.at[0]
+        send(None, own, dst, lat_yss.at[0], rs, i, mate, False)
 
     def lat_stage(d):
         for c in range(CHUNKS):
@@ -239,14 +255,24 @@
                 here = z - d >= 0 if sign < 0 else z + d < Z
                 onward = jnp.logical_and(here, z < Z - 1 if sign < 0 else z > 0)
                 piece = lat_piece(block, c)
-                rs = lat_rs.at[c, block]
-
-                def come(piece=piece, rs=rs, block=block, c=c):
-                    arrived(piece, lat_ss.at[c, block, 0], rs)
+                layer = z + d * sign
+                rs = lat_rs.at[c, layer]
+
+                def come(piece=piece, rs=rs):
+                    arrived(piece, lat_yss.at[0], rs)
 
                 when(here, come)
-                send(onward, piece, piece, lat_ss.at[c, block, 0], rs, i, t - 2 * sign)
-                send(here, piece, piece, lat_ss.at[c, block, 2], rs, i, mate)
+                send(onward, piece, piece, lat_ss.at[c, layer], rs, i, t - 2 * sign)
+                over = here
+                if d == 1 and c >= CHUNKS // 2:
+                    over = jnp.logical_and(here, even_layer if sign < 0 else jnp.logical_not(even_layer))
+                send(over, piece, piece, lat_yss.at[0], lat_yrs.at[0], i, mate, False)
+
+    def lat_cross():
+        for c in range(CHUNKS // 2, CHUNKS):
+            piece = lat_piece(mate, c)
+            arrived(piece, lat_yss.at[0], lat_rs.at[c, Z])
+            send(None, piece, piece, lat_ss.at[c, Z + 1], lat_yrs.at[0], i, paired)
 
     def silu(v):
         return v / (1.0 + jnp.exp(-v))
@@ -268,19 +294,20 @@
         two_lines(0, shift_ref, True) + two_lines(2, scale_ref, True) + two_lines(4, gate_ref, False)
     )[None]
     for k in range(1, S):
-        send(None, part.at[i], part.at[i], part_ss.at[k], part_rs.at[i], lax.rem(i + k, S), t)
+        send(None, part.at[i], part.at[i], part_ss.at[0], part_rs.at[0], lax.rem(i + k, S), t, False)
 
     lat_stage(1)
-
-    for k in range(1, S):
-        peer = lax.rem(i + k, S)
-        arrived(part.at[peer], part_ss.at[k], part_rs.at[peer])
+    lat_cross()
+
+    arrived(part.at[pl.ds(0, S - 1)], part_ss.at[0], part_rs.at[0])
     total = part[0]
     for k in range(1, S):
         total = total + part[k]
     terms[pl.ds(t, 1)] = total[None]
     for k in range(1, T):
-        send(None, terms.at[t], terms.at[t], term_ss.at[k], term_rs.at[t], i, lax.rem(t + k, T))
+        send(
+            None, terms.at[t], terms.at[t], term_ss.at[0], term_rs.at[0], i, lax.rem(t + k, T), False
+        )
 
     lane = lax.broadcasted_iota(jnp.int32, (count, VALUE), 1)
     place = i * count + lax.broadcasted_iota(jnp.int32, (count, VALUE), 0)
@@ -294,56 +321,66 @@
     tables[0] = jnp.cos(angle)
     tables[1] = jnp.sin(angle)
 
-    def wo_piece(block, share):
+    weight_step = VALUE // WEIGHT_CHUNKS
+
+    def wo_piece(block, share, w):
         return wo.at[
-            pl.ds(block * VALUE, VALUE),
+            pl.ds(block * VALUE + w * weight_step, weight_step),
             pl.ds(pl.multiple_of(share * quarter_cols, quarter_cols), quarter_cols),
         ]
 
-    def wo_twin(cond, block):
-        piece = wo_piece(block, core)
-        send(cond, piece, piece, wo_ss.at[block, 3], wo_rs.at[block, core], twin, t)
+    def wo_arrive(cond, block, rs, w):
+        def come():
+            arrived(wo_piece(block, core, w), wo_yss.at[0], rs)
+
+        when(cond, come)
+
+    def wo_send(cond, block, ss, rs, w, sp, tp, tracked=True):
+        piece = wo_piece(block, core, w)
+        send(cond, piece, piece, ss, rs, sp, tp, tracked)
+        if tracked:
+            late.append(pending.pop())
+
+    def wo_twin(cond, block, w):
+        wo_send(cond, block, wo_tss.at[0], wo_trs.at[0], w, twin, t, False)
 
     def wo_stage(d):
-        for sign in (-1, 1):
-            block = t + 2 * d * sign
-            here = z - d >= 0 if sign < 0 else z + d < Z
-            onward = jnp.logical_and(here, z < Z - 1 if sign < 0 else z > 0)
-            piece = wo_piece(block, core)
-            rs = wo_rs.at[block, core]
-
-            def come(piece=piece, rs=rs, block=block):
-                arrived(piece, wo_ss.at[block, 0], rs)
-
-            when(here, come)
-            send(onward, piece, piece, wo_ss.at[block, 0], rs, i, t - 2 * sign)
-            send(here, piece, piece, wo_ss.at[block, 2], rs, i, mate)
-            wo_twin(here, block)
+        for w in range(WEIGHT_CHUNKS):
+            for sign in (-1, 1):
+                layer = z + d * sign
+                block = t + 2 * d * sign
+                here = z - d >= 0 if sign < 0 else z + d < Z
+                onward = jnp.logical_and(here, z < Z - 1 if sign < 0 else z > 0)
+                wo_arrive(here, block, wo_rs.at[w, layer], w)
+                wo_send(onward, block, wo_ss.at[w, layer], wo_rs.at[w, layer], w, i, t - 2 * sign)
+                over = here
+                if d == 1 and w >= WEIGHT_CHUNKS // 2:
+                    over = jnp.logical_and(here, even_layer if sign < 0 else jnp.logical_not(even_layer))
+                wo_send(over, block, wo_yss.at[0], wo_mrs.at[w, layer], w, i, mate, False)
+                wo_twin(here, block, w)
 
     def wo_mate(d):
-        for sign in (-1, 1) if d else (1,):
-            block = mate + 2 * d * sign
-            here = None if not d else (z - d >= 0 if sign < 0 else z + d < Z)
-            piece = wo_piece(block, core)
-
-            def come(piece=piece, block=block):
-                arrived(piece, wo_ss.at[block, 0], wo_rs.at[block, core])
-
-            when(here, come)
-            wo_twin(here, block)
+        for w in range(WEIGHT_CHUNKS):
+            for sign in (-1, 1) if d else (1,):
+                layer = z + d * sign
+                block = mate + 2 * d * sign
+                here = None if not d else (z - d >= 0 if sign < 0 else z + d < Z)
+                wo_arrive(here, block, wo_mrs.at[w, layer], w)
+                if not d and w >= WEIGHT_CHUNKS // 2:
+                    wo_send(None, block, wo_ss.at[w, Z + 1], wo_mrs.at[w, z], w, i, paired)
+                wo_twin(here, block, w)
 
     loads[3].wait()
-    own_wo = wo_piece(t, core)
     for d in range(2, Z):
         lat_stage(d)
         if d == 2:
-            send(z < Z - 1, own_wo, own_wo, wo_ss.at[t, 0], wo_rs.at[t, core], i, t + 2)
-            send(z > 0, own_wo, own_wo, wo_ss.at[t, 1], wo_rs.at[t, core], i, t - 2)
-    send(None, own_wo, own_wo, wo_ss.at[t, 2], wo_rs.at[t, core], i, mate)
-
-    for k in range(1, T):
-        peer = lax.rem(t + k, T)
-        arrived(terms.at[peer], term_ss.at[k], term_rs.at[peer])
+            for w in range(WEIGHT_CHUNKS):
+                wo_send(z < Z - 1, t, wo_ss.at[w, z], wo_rs.at[w, z], w, i, t + 2)
+                wo_send(z > 0, t, wo_ss.at[w, Z], wo_rs.at[w, z], w, i, t - 2)
+    for w in range(WEIGHT_CHUNKS):
+        wo_send(None, t, wo_yss.at[0], wo_mrs.at[w, z], w, i, mate, False)
+
+    arrived(terms.at[pl.ds(0, T - 1)], term_ss.at[0], term_rs.at[0])
 
     def modulate_into(dst, src, first, n, which):
         wide = src[...].astype(f32)
@@ -370,15 +407,8 @@
     send(None, ckv_piece(i), ckv_piece(i), ckv_ss.at[0], ckv_rs.at[i], across, t)
     send(None, ckv_piece(i), ckv_piece(i), ckv_ss.at[1], ckv_rs.at[i], twin, t)
 
-    for d in range(Z):
-        for sign in (-1, 1) if d else (1,):
-            block = mate + 2 * d * sign
-            here = None if not d else (z - d >= 0 if sign < 0 else z + d < Z)
-            for c in range(CHUNKS):
-                def come(block=block, c=c):
-                    arrived(lat_piece(block, c), lat_ss.at[c, block, 0], lat_rs.at[c, block])
-
-                when(here, come)
+    over_rows = Z * rows - rows // 2
+    arrived(lat.at[pl.ds(0, over_rows), :], lat_yss.at[0], lat_yrs.at[0])
     lat[pl.ds(t * rows, rows), :] = lat_ref[...]
     modulate_into(mod, lat, 0, count, 0)
     projected = jnp.dot(mod[...], wqkv[...], preferred_element_type=f32)
@@ -395,7 +425,6 @@
     )
     send(None, kv_piece(i), kv_piece(i), kv_ss.at[0], kv_rs.at[i], across, t)
     send(None, kv_piece(i), kv_piece(i), kv_ss.at[1], kv_rs.at[i], twin, t)
-    wo_stage(1)
     arrived(ckv_piece(across), ckv_ss.at[2], ckv_rs.at[across])
     send(None, ckv_piece(across), ckv_piece(across), ckv_ss.at[2], ckv_rs.at[across], twin, t)
     query = rotated(projected[:, :VALUE]).astype(bf16) * jnp.asarray(HEAD ** (-0.5), bf16)
@@ -418,15 +447,15 @@
         )
 
     sums = attend(i)
+    wo_stage(1)
+    wo_mate(0)
     arrived(kv_piece(twin), kv_ss.at[2], kv_rs.at[twin])
     arrived(ckv_piece(twin), ckv_ss.at[2], ckv_rs.at[twin])
     sums = sums + attend(twin)
-    wo_mate(0)
-    wo_stage(2)
     arrived(kv_piece(across), kv_ss.at[2], kv_rs.at[across])
     send(None, kv_piece(across), kv_piece(across), kv_ss.at[2], kv_rs.at[across], twin, t)
+    wo_stage(2)
     sums = sums + attend(across)
-    wo_mate(1)
     arrived(kv_piece(twin_across), kv_ss.at[2], kv_rs.at[twin_across])
     arrived(ckv_piece(twin_across), ckv_ss.at[2], ckv_rs.at[twin_across])
     sums = sums + attend(twin_across)
@@ -439,25 +468,31 @@
     for k in range(1, T):
         peer = lax.rem(t + k, T)
         send(
-            None, ho_send.at[pl.ds(peer * rows, rows), :], ho.at[0, t], ho_ss.at[k], ho_rs.at[t], i, peer
+            None, ho_send.at[pl.ds(peer * rows, rows), :], ho.at[0, t], ho_ss.at[0], ho_rs.at[0], i, peer, False
         )
     for k in range(T):
         peer = lax.rem(t + k, T)
         send(
-            None, ho_send.at[pl.ds(peer * rows, rows), :], ho.at[1, t], hx_ss.at[k], hx_rs.at[t], across, peer
+            None, ho_send.at[pl.ds(peer * rows, rows), :], ho.at[1, t], hx_ss.at[0], hx_rs.at[0], across, peer, False
         )
     ho[0, pl.ds(t, 1)] = ho_send[pl.ds(t * rows, rows), :][None]
 
     for d in range(3, Z):
         wo_stage(d)
-    for d in range(2, Z):
+    drain()
+    sent_all(lat.at[pl.ds(0, over_rows), :], lat_yss.at[0])
+    sent_all(part.at[pl.ds(0, S - 1)], part_ss.at[0])
+    sent_all(terms.at[pl.ds(0, T - 1)], term_ss.at[0])
+    for d in range(1, Z):
         wo_mate(d)
-    for k in range(T):
-        peer = lax.rem(t + k, T)
-        if k:
-            arrived(wo_piece(peer, 1 - core), wo_ss.at[peer, 0], wo_rs.at[peer, 1 - core])
-            arrived(ho.at[0, peer], ho_ss.at[k], ho_rs.at[peer])
-        arrived(ho.at[1, peer], hx_ss.at[k], hx_rs.at[peer])
+    twin_rows = (T - 1) * VALUE
+    twin_view = wo.at[pl.ds(0, twin_rows), pl.ds(0, quarter_cols)]
+    arrived(twin_view, wo_tss.at[0], wo_trs.at[0])
+    pending[:] = late
+    drain()
+    sent_all(wo.at[pl.ds(0, Z * VALUE - weight_step), pl.ds(0, quarter_cols)], wo_yss.at[0])
+    arrived(ho.at[0, pl.ds(0, T - 1)], ho_ss.at[0], ho_rs.at[0])
+    arrived(ho.at[1], hx_ss.at[0], hx_rs.at[0])
     heads = jnp.concatenate(
         [jnp.concatenate([ho[which, h] for h in range(T)], axis=1) for which in (1, 0)], axis=0
     )
@@ -479,6 +514,9 @@
     for j in range(blocks):
         cols = pl.ds(pl.multiple_of(side * half + j * width, width), width)
         out_ref[:, cols] = (lat_ref[:, cols].astype(f32) + near[j]).astype(bf16)
+    sent_all(twin_view, wo_tss.at[0])
+    sent_all(ho.at[0, pl.ds(0, T - 1)], ho_ss.at[0])
+    sent_all(ho.at[1], hx_ss.at[0])
     for n in range(FAR_PIECES):
         piece = pl.ds(n * per_piece * width, per_piece * width)
         arrived(far_recv.at[:, piece], far_ss.at[n], far_rs.at[n])
@@ -489,11 +527,7 @@
                 + far_recv[:, j * width : (j + 1) * width].astype(f32)
             ).astype(bf16)
 
-    for cond, made in pending:
-        def finish(made=made):
-            made.wait_send()
-
-        when(cond, finish)
+    drain()
 
 
 def fused_shards(S, T, *args):
@@ -531,9 +565,12 @@
             pltpu.VMEM(shift_weight.shape, bf16),
             pltpu.VMEM((rows, D // 2), bf16),
             pltpu.VMEM((rows, D // 2), bf16),
-            dma((7,)), dma((CHUNKS, T, 3)), dma((CHUNKS, T)), dma((S,)), dma((S,)),
-            dma((T,)), dma((T,)), dma((3,)), dma((S,)), dma((3,)), dma((S,)),
-            dma((T,)), dma((T,)), dma((T,)), dma((T,)), dma((T, 4)), dma((T, 2)),
+            dma((7,)), dma((CHUNKS, T // 2 + 2)), dma((CHUNKS, T // 2 + 1)), dma((1,)), dma((1,)),
+            dma((1,)), dma((1,)), dma((1,)), dma((1,)),
+            dma((3,)), dma((S,)), dma((3,)), dma((S,)),
+            dma((1,)), dma((1,)), dma((1,)), dma((1,)),
+            dma((WEIGHT_CHUNKS, T // 2 + 2)), dma((WEIGHT_CHUNKS, T // 2)),
+            dma((WEIGHT_CHUNKS, T // 2)), dma((1,)), dma((1,)), dma((1,)),
             dma((FAR_PIECES,)), dma((FAR_PIECES,)),
         ],
         compiler_params=pltpu.CompilerParams(
@@ -550,8 +587,8 @@
     D = shapes[0][1]
     heads = shapes[8][1] // VALUE
     return (
-        S == 4 and T % (2 * FAR_PIECES) == 0 and heads == T and rows % (16 * CHUNKS) == 0
-        and crows % 16 == 0 and D % (128 * T) == 0 and T >= 8
+        S == 4 and T % (2 * FAR_PIECES) == 0 and heads == T and rows % 16 == 0
+        and crows % 16 == 0 and D % (128 * T) == 0 and D % (128 * CHUNKS) == 0 and T >= 8
         and rows * T * D * 8 + T * VALUE * D * 2 < 24 * 1024 * 1024
     )
 

time: 47 us -> 46.3 us (0.985)
  Pallas kernels: 44.6 us -> 43.9 us
    pallas_call x1, Pallas kernels: 44.6 us -> 43.9 us  [fused_shards(): pl.pallas_call(functools.partial(fused_kernel, S=S, T=T), out_shape=jax.S...]
where the time goes in v3:
time: 46.3 us; the launch traced here: 46.1 us
  Pallas kernels  43.9 us (95%)
  local copies, waits for them, and re-layouts  1.57 us (3%)
  between operations  0.66 us (1%)
    pallas_call x1, Pallas kernels, fused_shards(): pl.pallas_call(functools.partial(fused_kernel, S=S, T=T), out_shape=jax.S...  43.9 us
    unnamed x1, local copies, waits for them, and re-layouts  1.57 us

profile of v3, /device:TPU:0, one launch (start us, length us, event | category | flops | bytes accessed | tf_op | source)
XLA Modules:
  0.0 46.1 jit_solution(18019265372238286868)
XLA Ops:
  0.7 43.9 %shard_map.136 = bf16[32,2048]{1,0:T(8,128)(2,1)} custom-call(bf16[32,2048]{1,0:T(8,128)(2,1)} %lat_ref.1, bf16[64,2048]{1,0:T(8,128)(2,1)} %ctx_ref.1, f32[1,512]{1,0:T(1,128)} %bitcast.5, f32[1,512]{1,0:T(1,128)} %bitcast.6, f32[1,2048]{1,0:T(1,128)} %bitcast.4, bf16[512,256]{1,0:T(8,128)(2,1)} %shift_hbm.1, bf16[512,256]{1,0:T(8,128)(2,1)} %scale_hbm.1, ...), custom_call_target="tpu_custom_call" | custom-call | tf_op jit(solution)/shard_map/pallas_call | solution.py:545
  44.6 1.6 %copy.17 = bf16[32,2048]{1,0:T(8,128)(2,1)} copy(bf16[32,2048]{1,0:T(8,128)(2,1)} %shard_map.136) | data formatting | bytes 262144
